TPU v7x, 32 devices: a whole 2x2x4 slice. The times are simulated.
32 devices in a mesh: grp: 2 (over x), ep: 4 (over y, core), tp: 4 (over z).
Axes of the slice: x: 2, y: 2, z: 4, core: 2. Of those that a mesh axis runs over, the one named last changes fastest.
Arguments:
- tokens: bfloat16 [4096, 1024], P(('grp', 'ep', 'tp')), parts along dimension 0, may hold values from -6 to 6
- norm_gain: float32 [1024], replicated, may hold values from 0.1 to 1.9
- gate_weight: bfloat16 [4, 1024, 3584], P('ep', None, 'tp'), may hold values from -0.1875 to 0.1875
- up_weight: bfloat16 [4, 1024, 3584], P('ep', None, 'tp'), may hold values from -0.1875 to 0.1875
- down_weight: bfloat16 [4, 3584, 1024], P('ep', 'tp'), may hold values from -0.09375 to 0.09375
- expert_ids: int32 [4096, 2], P(('grp', 'ep')), parts along dimension 0, may hold values from 0 to 3, all different within a row; in each aligned block of 128 rows (0 to 127, 128 to 255, ...) at most 80 rows name the same one
- route_weight: float32 [4096, 2], P(('grp', 'ep')), parts along dimension 0, may hold values from 0.2 to 1
Outputs:
- mixed: bfloat16 [4096, 1024], P(('grp', 'ep', 'tp')), parts along dimension 0
There are 2 independent parts, one for each index of `grp`. A program takes and returns all parts, laid end to end along the dimension named above; an argument that names none is the same for every part. Nothing has to cross between parts.
Inputs may be any that keep to these rules, and one draw needn't show every extreme that they name: `expert_ids`: A token's 2 experts differ. In the rows of one device (128 tokens, aligned blocks) no expert is named more than 80 times, and in every draw some expert is named exactly 80 times in some device's rows.
All inputs are finite; a program needn't handle non-finite values.
Results may differ from a plain program's by a relative error of at most 0.015.
Values may be sent and summed in bfloat16 or wider, within the bound.
A program may use at most 64 MiB of HBM per device.

v0:
```python
import jax
import jax.numpy as jnp
from jax import lax
from jax.sharding import PartitionSpec as P

TOP_K = 2


def norm_rows(tokens, norm_gain):
    values = tokens.astype(jnp.float32)
    scaled = values * lax.rsqrt(jnp.mean(values * values, axis=-1, keepdims=True) + 1e-06)
    return (scaled * norm_gain).astype(jnp.bfloat16)


def expert_hidden(rows, gate_weight, up_weight):
    gate = jnp.einsum("e...d,edf->e...f", rows, gate_weight, preferred_element_type=jnp.float32)
    upper = jnp.einsum("e...d,edf->e...f", rows, up_weight, preferred_element_type=jnp.float32)
    return (jax.nn.silu(gate) * upper).astype(jnp.bfloat16)


def weigh_pieces(summed, weights):
    piece = lax.optimization_barrier(summed.astype(jnp.bfloat16)).astype(jnp.float32)
    total = piece[:, 0] * weights[:, 0:1]
    total = total + piece[:, 1] * weights[:, 1:2]
    return total.astype(jnp.bfloat16)


def body(tokens, norm_gain, gate_weight, up_weight, down_weight, expert_ids, route_weight):
    tok_rows = tokens.shape[0]
    width = tokens.shape[1]
    local_experts = gate_weight.shape[0]
    inner = gate_weight.shape[2]
    n_tp = lax.axis_size("tp")
    n_ep = lax.axis_size("ep")
    experts = n_ep * local_experts
    most = max(2, tok_rows * TOP_K * 5 // (4 * experts))
    normed = norm_rows(tokens, norm_gain)
    flat_ids = expert_ids.reshape(n_tp, tok_rows * TOP_K)
    onehot = (flat_ids[:, :, None] == jnp.arange(experts, dtype=jnp.int32)[None, None, :]).astype(
        jnp.int32
    )
    before = jnp.cumsum(onehot, axis=1) - onehot
    slots = jnp.sum(before * onehot, axis=-1)
    owner = jnp.arange(n_tp, dtype=jnp.int32)[:, None]
    row_index = (flat_ids * (n_tp * most) + owner * most + slots).reshape(-1)
    mine = lax.axis_index("tp")
    own_ids = lax.dynamic_slice_in_dim(flat_ids, mine, 1, 0)[0]
    own_slots = lax.dynamic_slice_in_dim(slots, mine, 1, 0)[0]
    own_index = own_ids * most + own_slots
    whole = lax.all_gather(normed, "tp", axis=0, tiled=True)
    sending = (
        jnp.zeros((experts * n_tp * most, width), jnp.bfloat16)
        .at[row_index]
        .set(jnp.repeat(whole, TOP_K, axis=0))
    )
    arrived = lax.all_to_all(
        sending.reshape(experts, n_tp * most, width), "ep", split_axis=0, concat_axis=1, tiled=True
    )
    hidden = expert_hidden(arrived, gate_weight, up_weight)
    by_source = hidden.reshape(local_experts, n_ep, n_tp, most, inner).transpose(2, 0, 1, 3, 4)
    per_device = local_experts * n_ep * most
    product = jnp.einsum(
        "tlnmf,lfd->tlnmd", by_source, down_weight, preferred_element_type=jnp.float32
    )
    own_sums = lax.psum_scatter(
        product.astype(jnp.bfloat16)
        .astype(jnp.float32)
        .reshape(per_device * lax.axis_size("tp"), width)
        .astype(jnp.bfloat16),
        "tp",
        scatter_dimension=0,
        tiled=True,
    )
    own_pieces = own_sums.reshape(local_experts, n_ep, most, width)
    back = lax.all_to_all(own_pieces, "ep", split_axis=1, concat_axis=0, tiled=True)
    picked = back.reshape(experts * most, width)[own_index].reshape(tok_rows, TOP_K, width)
    own_weights = lax.dynamic_slice_in_dim(route_weight, mine * tok_rows, tok_rows, 0)
    return weigh_pieces(picked.astype(jnp.float32), own_weights)


def solution(mesh):
    placed = (
        P(("grp", "ep", "tp"), None),
        P(),
        P("ep", None, "tp"),
        P("ep", None, "tp"),
        P("ep", "tp", None),
        P(("grp", "ep"), None),
        P(("grp", "ep"), None),
    )
    return jax.shard_map(
        body, mesh=mesh, in_specs=placed, out_specs=P(("grp", "ep", "tp"), None), check_vma=False
    )
```

profile of v0, /device:TPU:0, one launch (start us, length us, event | category | flops | bytes accessed | tf_op | source)
XLA Modules:
  0.0 175.1 jit_solution(9115323887574914538)
XLA Ops:
  6.5 1.2 fusion.12
  7.8 1.8 %fusion.14 = bf16[128,1024]{1,0:T(8,128)(2,1)} fusion(bf16[128,1024]{1,0:T(8,128)(2,1)} %param.7, f32[1024]{0:T(1024)} %param.8, f32[128]{0:T(128)S(1)} %add_rsqrt_fusion), kind=kLoop, calls=%fused_computation.17 | loop fusion | flops 524288 | bytes 528896 | tf_op jit(solution)/shard_map/convert_element_type | solution.py:12
  9.6 0.8 copy.20
  10.5 0.2 eq.29
  10.6 0.2 eq.25
  10.8 4.8 %reduce-window.6 = s32[4,4,2,128]{3,2,1,0:T(2,128)S(1)} reduce-window(s32[4,4,2,128]{3,2,1,0:T(2,128)S(1)} %compare_convert_fusion, s32[]{:T(128)} %constant.16.clone.1), window={size=1x1x1x128 pad=0_0x0_0x0_0x127_0}, to_apply=%region_0.0 | reduce-window | flops 520192 | bytes 32772 | tf_op jit(solution)/shard_map/reduce-window
  16.2 0.7 broadcast_multiply_fusion
  16.9 0.1 copy.19
  17.0 0.2 mul.95
  17.3 23.1 %all-gather.2.cloned.1.call-done = bf16[512,1024]{1,0:T(8,128)(2,1)} async-done(((bf16[128,1024]{1,0:T(8,128)(2,1)}), bf16[512,1024]{1,0:T(8,128)(2,1)}) %all-gather.2.cloned.1.call-update) | async-done | bytes 1048592 | tf_op jit(solution)/shard_map/all_gather | solution.py:50
  40.4 3.7 %broadcast_in_dim.5 = bf16[512,2,1024]{2,1,0:T(2,128)(2,1)} broadcast(bf16[512,1024]{1,0:T(8,128)(2,1)} %all-gather.2.cloned.1.call-done), dimensions={0,2} | broadcast | bytes 3145728 | tf_op jit(solution)/shard_map/broadcast_in_dim | solution.py:54
  44.1 4.1 %reshape.185 = bf16[1024,1024]{1,0:T(8,128)(2,1)} reshape(bf16[512,2,1024]{2,1,0:T(2,128)(2,1)} %broadcast_in_dim.5) | data formatting | bytes 4194304 | tf_op jit(solution)/shard_map/reshape | solution.py:54
  48.2 7.8 %scatter_custom_fusion = bf16[1280,1024]{1,0:T(8,128)(2,1)} fusion(s32[1024]{0:T(1024)S(1)} %bitcast.84, bf16[1024,1024]{1,0:T(8,128)(2,1)} %reshape.185, bf16[]{:T(256)} %constant.13.clone.1), kind=kCustom, calls=%fused_computation.11 | custom fusion | bytes 2621952 | tf_op jit(solution)/shard_map/scatter | solution.py:54
  56.0 35.0 %all_to_all.8 = bf16[4,320,1024]{2,1,0:T(8,128)(2,1)S(1)} all-to-all(bf16[4,320,1024]{2,1,0:T(8,128)(2,1)} %bitcast.75), channel_id=1, replica_groups=mesh['grp'=2,'ep'=4,'tp'=4] {'ep'}, dimensions={0} | all-to-all | bytes 5242880 | tf_op jit(solution)/shard_map/all_to_all | solution.py:56
  91.0 2.9 %fusion.8 = f32[1280,896]{1,0:T(8,128)S(1)} fusion(bf16[1280,1024]{1,0:T(8,128)(2,1)S(1)} %bitcast.77, bf16[1,1024,896]{2,1,0:T(8,128)(2,1)S(1)} %copy-done.1), kind=kOutput, calls=%fused_computation.9 | convolution fusion | flops 2348810240 | bytes 9043968 | tf_op jit(solution)/shard_map/e...d,edf->e...f/dot_general | solution.py:16
  94.0 3.2 %multiply_convert_fusion = bf16[1280,896]{1,0:T(8,128)(2,1)S(1)} fusion(f32[1280,896]{1,0:T(8,128)S(1)} %fusion.8, bf16[1280,1024]{1,0:T(8,128)(2,1)S(1)} %bitcast.78, bf16[1,1024,896]{2,1,0:T(8,128)(2,1)S(1)} %copy-done.2), kind=kOutput, calls=%fused_computation.2 | convolution fusion | flops 2355691520 | bytes 11337728 | tf_op jit(solution)/shard_map/e...d,edf->e...f/dot_general | solution.py:17
  97.2 4.2 %fusion.3 = bf16[4,4,80,1024]{3,2,1,0:T(8,128)(2,1)} fusion(bf16[1,4,4,80,896]{4,3,2,1,0:T(8,128)(2,1)S(1)} %bitcast.85, bf16[1,896,1024]{2,1,0:T(8,128)(2,1)S(1)} %copy-done), kind=kOutput, calls=%fused_computation.6 | convolution fusion | flops 2350120960 | bytes 6750208 | tf_op jit(solution)/shard_map/tlnmf,lfd->tlnmd/dot_general | solution.py:62
  101.4 50.9 %reduce-scatter.2.cloned.1.call-done = bf16[320,1024]{1,0:T(8,128)(2,1)} async-done(((bf16[1280,1024]{1,0:T(8,128)(2,1)}), bf16[320,1024]{1,0:T(8,128)(2,1)}) %reduce-scatter.2.cloned.1.call-update) | async-done | bytes 655376 | tf_op jit(solution)/shard_map/reduce_scatter | solution.py:65
  152.2 3.5 %all-to-all-start.1 = ((bf16[1,4,80,1024]{3,2,0,1:T(8,128)(2,1)}), bf16[1,4,80,1024]{3,2,0,1:T(8,128)(2,1)S(1)}, u32[]{:S(2)}, u32[]{:S(2)}) async-start(bf16[1,4,80,1024]{3,2,0,1:T(8,128)(2,1)} %bitcast.79), calls=%async_computation.2 | async-start | bytes 1310720 | tf_op jit(solution)/shard_map/all_to_all | solution.py:75
  155.7 0.7 constant_dynamic-slice_fusion
  156.4 9.5 %all-to-all-done.1 = bf16[1,4,80,1024]{3,2,0,1:T(8,128)(2,1)S(1)} async-done(((bf16[1,4,80,1024]{3,2,0,1:T(8,128)(2,1)}), bf16[1,4,80,1024]{3,2,0,1:T(8,128)(2,1)S(1)}, u32[]{:S(2)}, u32[]{:S(2)}) %all-to-all-start.1) | async-done | bytes 655392 | tf_op jit(solution)/shard_map/all_to_all | solution.py:75
  165.9 1.2 gather_fusion
  167.1 0.2 reshape.172
  167.4 0.8 fusion.17
  (29 shorter events, 0.8 us)
Async XLA Ops:
  6.5 90.6 %copy-start = (bf16[1,896,1024]{2,1,0:T(8,128)(2,1)S(1)}, bf16[1,896,1024]{2,1,0:T(8,128)(2,1)}, u32[]{:S(2)}) copy-start(bf16[1,896,1024]{2,1,0:T(8,128)(2,1)} %param.11) | copy-start | bytes 5505028
  6.5 33.9 %all-gather.2.cloned.1.call-start = ((), (), s32[]{:S(2)}) async-start(), calls=%async_computation.3 | async-start | bytes 1310720 | tf_op jit(solution)/shard_map/all_gather | solution.py:50
  9.6 142.6 %reduce-scatter.2.cloned.1.call-start = ((), (), s32[]{:S(2)}) async-start(), calls=%async_computation.4 | async-start | bytes 3276800 | tf_op jit(solution)/shard_map/reduce_scatter | solution.py:65
  56.0 35.0 %copy-start.1 = (bf16[1,1024,896]{2,1,0:T(8,128)(2,1)S(1)}, bf16[1,1024,896]{2,1,0:T(8,128)(2,1)}, u32[]{:S(2)}) copy-start(bf16[1,1024,896]{2,1,0:T(8,128)(2,1)} %param.9) | copy-start | bytes 5505028
  91.0 2.9 %copy-start.2 = (bf16[1,1024,896]{2,1,0:T(8,128)(2,1)S(1)}, bf16[1,1024,896]{2,1,0:T(8,128)(2,1)}, u32[]{:S(2)}) copy-start(bf16[1,1024,896]{2,1,0:T(8,128)(2,1)} %param.10) | copy-start | bytes 5505028
  152.2 13.7 %all-to-all-start.1 = ((bf16[1,4,80,1024]{3,2,0,1:T(8,128)(2,1)}), bf16[1,4,80,1024]{3,2,0,1:T(8,128)(2,1)S(1)}, u32[]{:S(2)}, u32[]{:S(2)}) async-start(bf16[1,4,80,1024]{3,2,0,1:T(8,128)(2,1)} %bitcast.79), calls=%async_computation.2 | async-start | bytes 1310720 | tf_op jit(solution)/shard_map/all_to_all | solution.py:75
Sparse Core Ops, SparseCore 0:
  9.7 30.6 all-gather.1
  101.5 50.6 reduce-scatter.1
where the time goes:
time: 176 us; the launch traced here: 175 us
  waiting for transfers between devices  83.5 us (47%)
  blocking collectives  35 us (20%)
  local copies, waits for them, and re-layouts  19.6 us (11%)
  between operations  13.5 us (8%)
  matrix products  10.2 us (6%)
  other arithmetic  9.67 us (5%)
  starting transfers between devices  3.53 us (2%)
    reduce_scatter x1, waiting for transfers between devices, body(): lax.psum_scatter(product.astype(jnp.bfloat16).astype(jnp.float32).reshape...  50.9 us
    all_to_all x1, blocking collectives, body(): lax.all_to_all(sending.reshape(experts, n_tp * most, width), 'ep', split_...  35 us
    all_gather x1, waiting for transfers between devices, body(): whole = lax.all_gather(normed, 'tp', axis=0, tiled=True)  23.1 us
    all_to_all x1, waiting for transfers between devices, body(): lax.all_to_all(own_pieces, 'ep', split_axis=1, concat_axis=0, tiled=True)  9.46 us
    scatter x1, local copies, waits for them, and re-layouts, body(): sending = jnp.zeros((experts * n_tp * most, width), jnp.bfloat16).at[row_...  7.78 us
    another operation x3, other arithmetic  4.92 us
    dot_general x1, matrix products, body(): jnp.einsum('tlnmf,lfd->tlnmd', by_source, down_weight, preferred_element_...  4.17 us
    reshape x1, local copies, waits for them, and re-layouts, body(): jnp.repeat(whole, TOP_K, axis=0)  4.12 us
  transfers between devices with their start and end apart: 3, of which 3 were waited for; matrix products, arithmetic and copies ran while one was open for 5% of the time, Pallas kernels for 0%

commit v1 on v0

--- a/solution.py
+++ b/solution.py
@@ -1,9 +1,15 @@
+import functools
+
 import jax
 import jax.numpy as jnp
 from jax import lax
+from jax.experimental import pallas as pl
+from jax.experimental.pallas import tpu as pltpu
 from jax.sharding import PartitionSpec as P
 
 TOP_K = 2
+MESH = pl.DeviceIdType.MESH
+VMEM_ROOM = 48 << 20
 
 
 def norm_rows(tokens, norm_gain):
@@ -25,7 +31,7 @@
     return total.astype(jnp.bfloat16)
 
 
-def body(tokens, norm_gain, gate_weight, up_weight, down_weight, expert_ids, route_weight):
+def plain_body(tokens, norm_gain, gate_weight, up_weight, down_weight, expert_ids, route_weight):
     tok_rows = tokens.shape[0]
     width = tokens.shape[1]
     local_experts = gate_weight.shape[0]
@@ -78,6 +84,229 @@
     return weigh_pieces(picked.astype(jnp.float32), own_weights)
 
 
+def place(step, n):
+    last = step // (2 * n - 1)
+    later = (step + 2 * n - 2) // (2 * n - 1)
+    dy = ((step + 1) % 2) * later + last
+    dz = (1 - dy) * ((step + 1) // 2) + dy * (step // 2 - 1 + last)
+    return dy, dz
+
+
+def step_of(dy, dz, n):
+    if dy == 0:
+        return 2 * dz - 1 if dz else 0
+    return 2 * n - 1 if dz == n - 1 else 2 * dz + 2
+
+
+def kernel(
+    n, tok_ref, gain_ref, share_ref, gate_hbm, up_hbm, down_hbm, out_ref,
+    gate, up, down, buf, shares, part, srecv, yrecv, zrecv, tbuf,
+    load_sem, w_s, w_r, agz_s, agz_r, agy_s, agy_r, ags_s, ags_r, rss_s, rss_r, rsy_s, rsy_r, rsz_s, rsz_r,
+):
+    ep = lax.axis_index("ep")
+    z = lax.axis_index("tp")
+    y, c = ep // 2, ep % 2
+    rows, width = tok_ref.shape
+    steps = 2 * n
+    sib = {"ep": 2 * y + 1 - c}
+    across = {"ep": 2 * (1 - y) + c}
+
+    def along(k):
+        return {"tp": (z + k) % n}
+
+    def remote(src, dst, send, recv, to):
+        return pltpu.make_async_remote_copy(
+            src_ref=src, dst_ref=dst, send_sem=send, recv_sem=recv, device_id=to, device_id_type=MESH
+        )
+
+    loads = [
+        pltpu.make_async_copy(src.at[0], dst, load_sem.at[i])
+        for i, (src, dst) in enumerate(((gate_hbm, gate), (up_hbm, up), (down_hbm, down)))
+    ]
+    for load in loads:
+        load.start()
+
+    barrier = pltpu.get_barrier_semaphore()
+    for k in range(1, 4):
+        pl.semaphore_signal(barrier, inc=1, device_id={"ep": (ep + k) % 4}, device_id_type=MESH)
+    for k in range(1, n):
+        pl.semaphore_signal(barrier, inc=1, device_id=along(k), device_id_type=MESH)
+    buf[z, y, c] = norm_rows(tok_ref[...], gain_ref[...])
+    pl.semaphore_wait(barrier, 3 + n - 1)
+
+    def ag_sib(step):
+        dy, dz = place(step, n)
+        yb, zb = (y + dy) % 2, (z + dz) % n
+        return remote(buf.at[zb, yb, c], buf.at[zb, yb, c], ags_s.at[step], ags_r.at[step], sib)
+
+    def ag_y(dz):
+        zb = (z + dz) % n
+        return remote(buf.at[zb, y, c], buf.at[zb, y, c], agy_s.at[dz], agy_r.at[dz], across)
+
+    def ag_z(k):
+        return remote(buf.at[z, y, c], buf.at[z, y, c], agz_s.at[k], agz_r.at[n - k], along(k))
+
+    def share(k):
+        to = (ep + k) % 4
+        return remote(share_ref.at[to], shares.at[ep], w_s.at[k], w_r.at[4 - k], {"ep": to})
+
+    def rs_sib(step):
+        return remote(part.at[step, 1 - c], srecv.at[step], rss_s.at[step], rss_r.at[step], sib)
+
+    def rs_y(dz, step):
+        return remote(part.at[step, c], yrecv.at[dz], rsy_s.at[dz], rsy_r.at[dz], across)
+
+    def rs_z(dz):
+        return remote(tbuf.at[dz - 1], zrecv.at[n - dz - 1], rsz_s.at[dz], rsz_r.at[n - dz], along(dz))
+
+    ag_y(0).start()
+    for k in range(1, n):
+        ag_z(k).start()
+    for k in range(1, 4):
+        share(k).start()
+    shares[ep] = share_ref[ep]
+    for k in range(1, 4):
+        remote(share_ref.at[0], shares.at[(ep + k) % 4], w_s.at[k], w_r.at[k], sib).wait_recv()
+    for load in loads:
+        load.wait()
+
+    def arrive(step):
+        dy, dz = place(step, n)
+        yb, zb = (y + dy) % 2, (z + dz) % n
+        here = buf.at[zb, yb, c]
+
+        @pl.when(dy == 1)
+        def _():
+            remote(here, here, agy_s.at[dz], agy_r.at[dz], across).wait_recv()
+
+        @pl.when((dy == 0) & (dz > 0))
+        def _():
+            remote(here, here, agz_s.at[dz], agz_r.at[dz], sib).wait_recv()
+            ag_y(dz).start()
+
+        ag_sib(step).start()
+
+    def combine(step):
+        dy, dz = place(step, n)
+        rs_sib(step).wait_recv()
+        part[step, c] = (part[step, c].astype(jnp.float32) + srecv[step].astype(jnp.float32)).astype(jnp.bfloat16)
+
+        @pl.when((dy == 1) & (dz > 0))
+        def _():
+            rs_y(dz, step).start()
+
+    def column(row):
+        return jnp.transpose(jnp.broadcast_to(row, (rows, rows)))[:, :1]
+
+    def one(step, carry):
+        dy, dz = place(step, n)
+        yb, zb = (y + dy) % 2, (z + dz) % n
+        arrive(step)
+        theirs = buf.at[zb, yb, 1 - c]
+        remote(theirs, theirs, ags_s.at[step], ags_r.at[step], sib).wait_recv()
+        x = buf[zb, yb].reshape(2 * rows, width)
+        g = jnp.dot(x, gate[...], preferred_element_type=jnp.float32)
+        u = jnp.dot(x, up[...], preferred_element_type=jnp.float32)
+        hidden = (jax.nn.silu(g) * u).astype(jnp.bfloat16)
+        product = jnp.dot(hidden, down[...], preferred_element_type=jnp.float32)
+        for half in range(2):
+            w = column(shares[2 * yb + half, pl.ds(zb, 1), :])
+            part[step, half] = (product[half * rows : (half + 1) * rows] * w).astype(jnp.bfloat16)
+        rs_sib(step).start()
+
+        @pl.when(step > 0)
+        def _():
+            combine(step - 1)
+
+        return carry
+
+    lax.fori_loop(0, steps, one, 0)
+    combine(steps - 1)
+    rs_y(0, step_of(1, 0, n)).start()
+
+    def total(dz):
+        landed = yrecv.at[dz]
+        remote(landed, landed, rsy_s.at[dz], rsy_r.at[dz], across).wait_recv()
+        return part[step_of(0, dz, n), c].astype(jnp.float32) + yrecv[dz].astype(jnp.float32)
+
+    for dz in range(1, n):
+        tbuf[dz - 1] = total(dz).astype(jnp.bfloat16)
+        rs_z(dz).start()
+    result = total(0)
+    for dz in range(1, n):
+        landed = zrecv.at[dz - 1]
+        remote(landed, landed, rsz_s.at[dz], rsz_r.at[dz], sib).wait_recv()
+        result = result + zrecv[dz - 1].astype(jnp.float32)
+    out_ref[...] = result.astype(out_ref.dtype)
+
+    for k in range(1, 4):
+        share(k).wait_send()
+    for k in range(1, n):
+        ag_z(k).wait_send()
+        rs_z(k).wait_send()
+    for dz in range(n):
+        ag_y(dz).wait_send()
+        rs_y(dz, step_of(1, dz, n)).wait_send()
+    for step in range(steps):
+        ag_sib(step).wait_send()
+        rs_sib(step).wait_send()
+
+
+def kernel_bytes(n, rows, width, inner):
+    blocks = n * 4 + 2 * n * 2 + 2 * n + n + 2 * (n - 1) + 8
+    return 2 * width * (3 * inner + blocks * rows) + 16 * rows * (width + 2 * inner)
+
+
+def fused_body(tokens, norm_gain, gate_weight, up_weight, down_weight, expert_ids, route_weight):
+    rows, width = tokens.shape
+    inner = gate_weight.shape[2]
+    n = lax.axis_size("tp")
+    experts = lax.axis_size("ep")
+    named = expert_ids[None, :, :] == jnp.arange(experts, dtype=jnp.int32)[:, None, None]
+    share = jnp.sum(jnp.where(named, route_weight[None, :, :], 0.0), axis=-1).reshape(experts, n, rows)
+    vmem = pl.BlockSpec(memory_space=pltpu.VMEM)
+    anywhere = pl.BlockSpec(memory_space=pl.ANY)
+    dma = pltpu.SemaphoreType.DMA
+    bf16 = jnp.bfloat16
+    return pl.pallas_call(
+        functools.partial(kernel, n),
+        out_shape=jax.ShapeDtypeStruct((rows, width), bf16),
+        in_specs=[vmem] * 3 + [anywhere] * 3,
+        out_specs=vmem,
+        scratch_shapes=[
+            pltpu.VMEM((width, inner), bf16),
+            pltpu.VMEM((width, inner), bf16),
+            pltpu.VMEM((inner, width), bf16),
+            pltpu.VMEM((n, 2, 2, rows, width), bf16),
+            pltpu.VMEM((experts, n, rows), jnp.float32),
+            pltpu.VMEM((2 * n, 2, rows, width), bf16),
+            pltpu.VMEM((2 * n, rows, width), bf16),
+            pltpu.VMEM((n, rows, width), bf16),
+            pltpu.VMEM((n - 1, rows, width), bf16),
+            pltpu.VMEM((n - 1, rows, width), bf16),
+            dma((3,)),
+        ]
+        + [dma((4,))] * 2
+        + [dma((n,))] * 4
+        + [dma((2 * n,))] * 4
+        + [dma((n,))] * 4,
+        compiler_params=pltpu.CompilerParams(
+            collective_id=0, has_side_effects=True, vmem_limit_bytes=VMEM_ROOM
+        ),
+    )(tokens, norm_gain.reshape(1, width), share, gate_weight, up_weight, down_weight)
+
+
+def body(tokens, norm_gain, gate_weight, up_weight, down_weight, expert_ids, route_weight):
+    rows, width = tokens.shape
+    inner = gate_weight.shape[2]
+    n = lax.axis_size("tp")
+    fits = kernel_bytes(n, rows, width, inner) <= VMEM_ROOM
+    chosen = plain_body
+    if lax.axis_size("ep") == 4 and gate_weight.shape[0] == 1 and n > 1 and fits:
+        chosen = fused_body
+    return chosen(tokens, norm_gain, gate_weight, up_weight, down_weight, expert_ids, route_weight)
+
+
 def solution(mesh):
     placed = (
         P(("grp", "ep", "tp"), None),

time: 176 us -> 84.1 us (0.48)
  waiting for transfers between devices: 83.5 us -> 0 us
  Pallas kernels: 0 us -> 76.2 us
  blocking collectives: 35 us -> 0 us
  between operations: 13.5 us -> 0.02 us
  local copies, waits for them, and re-layouts: 19.6 us -> 6.85 us
  matrix products: 10.2 us -> 0 us
  other arithmetic: 9.67 us -> 0.72 us
  starting transfers between devices: 3.53 us -> 0 us
    pallas_call x0 -> x1, Pallas kernels: none -> 76.2 us  [fused_body(): pl.pallas_call(functools.partial(kernel, n), out_shape=jax.ShapeDtypeStru...]
    reduce_scatter x1 -> x0, waiting for transfers between devices: 50.9 us -> none  [body(): lax.psum_scatter(product.astype(jnp.bfloat16).astype(jnp.float32).reshape...]
    all_to_all x1 -> x0, blocking collectives: 35 us -> none  [body(): lax.all_to_all(sending.reshape(experts, n_tp * most, width), 'ep', split_...]
    all_gather x1 -> x0, waiting for transfers between devices: 23.1 us -> none  [body(): whole = lax.all_gather(normed, 'tp', axis=0, tiled=True)]
    dot_general x3 -> x0, matrix products: 10.2 us -> none  [the longest x1 4.17 us: body(): jnp.einsum('tlnmf,lfd->tlnmd', by_source, down_weight, preferred_element_...]
    all_to_all x1 -> x0, waiting for transfers between devices: 9.46 us -> none  [body(): lax.all_to_all(own_pieces, 'ep', split_axis=1, concat_axis=0, tiled=True)]
    scatter x1 -> x0, local copies, waits for them, and re-layouts: 7.78 us -> none  [body(): sending = jnp.zeros((experts * n_tp * most, width), jnp.bfloat16).at[row_...]
    unnamed x10 -> x11, local copies, waits for them, and re-layouts: 0.92 us -> 6.83 us
  transfers between devices with their start and end apart: 3 -> 0, of which waited for: 3 -> 0; matrix products, arithmetic and copies ran while one was open for 5% -> 0% of each run, Pallas kernels for 0% -> 0%
where the time goes in v1:
time: 84.1 us; the launch traced here: 83.8 us
  Pallas kernels  76.2 us (91%)
  local copies, waits for them, and re-layouts  6.85 us (8%)
    pallas_call x1, Pallas kernels, fused_body(): pl.pallas_call(functools.partial(kernel, n), out_shape=jax.ShapeDtypeStru...  76.2 us
    unnamed x11, local copies, waits for them, and re-layouts  6.83 us

profile of v1, /device:TPU:0, one launch (start us, length us, event | category | flops | bytes accessed | tf_op | source)
XLA Modules:
  0.0 83.8 jit_solution(10058008952807060124)
XLA Ops:
  0.0 0.7 select_reduce_fusion
  0.7 0.0 copy-start
  0.7 1.5 %copy-done = bf16[1,1024,896]{2,1,0:T(8,128)(2,1)S(1)} copy-done((bf16[1,1024,896]{2,1,0:T(8,128)(2,1)S(1)}, bf16[1,1024,896]{2,1,0:T(8,128)(2,1)}, u32[]{:S(2)}) %copy-start) | copy-done | bytes 1835032
  2.2 0.0 copy-start.1
  2.2 1.5 %copy-done.1 = bf16[1,1024,896]{2,1,0:T(8,128)(2,1)S(1)} copy-done((bf16[1,1024,896]{2,1,0:T(8,128)(2,1)S(1)}, bf16[1,1024,896]{2,1,0:T(8,128)(2,1)}, u32[]{:S(2)}) %copy-start.1) | copy-done | bytes 1835032
  3.7 0.0 copy-start.2
  3.7 1.5 %copy-done.2 = bf16[1,896,1024]{2,1,0:T(8,128)(2,1)S(1)} copy-done((bf16[1,896,1024]{2,1,0:T(8,128)(2,1)S(1)}, bf16[1,896,1024]{2,1,0:T(8,128)(2,1)}, u32[]{:S(2)}) %copy-start.2) | copy-done | bytes 1835032
  5.2 0.0 copy-start.3
  5.2 0.9 %copy-done.3 = bf16[128,1024]{1,0:T(8,128)(2,1)S(1)} copy-done((bf16[128,1024]{1,0:T(8,128)(2,1)S(1)}, bf16[128,1024]{1,0:T(8,128)(2,1)}, u32[]{:S(2)}) %copy-start.3) | copy-done | bytes 262168
  6.2 0.0 copy-start.4
  6.2 0.7 copy-done.4
  6.9 76.2 %shard_map.73 = bf16[128,1024]{1,0:T(8,128)(2,1)S(1)} custom-call(bf16[128,1024]{1,0:T(8,128)(2,1)S(1)} %copy-done.3, f32[1,1024]{1,0:T(1,128)S(1)} %bitcast.1, f32[4,4,128]{2,1,0:T(4,128)S(1)} %reshape.9.share_ref, bf16[1,1024,896]{2,1,0:T(8,128)(2,1)S(1)} %copy-done, bf16[1,1024,896]{2,1,0:T(8,128)(2,1)S(1)} %copy-done.1, bf16[1,896,1024]{2,1,0:T(8,128)(2,1)S(1)} %copy-done.2), custom_call_target="tpu_custom_call" | custom-call | tf_op jit(solution)/shard_map/pallas_call | solution.py:271
  83.1 0.7 copy.11
  (1 shorter events, 0.0 us)
Async XLA Ops:
  0.7 1.5 %copy-start = (bf16[1,1024,896]{2,1,0:T(8,128)(2,1)S(1)}, bf16[1,1024,896]{2,1,0:T(8,128)(2,1)}, u32[]{:S(2)}) copy-start(bf16[1,1024,896]{2,1,0:T(8,128)(2,1)} %gate_hbm.1) | copy-start | bytes 5505028
  2.2 1.5 %copy-start.1 = (bf16[1,1024,896]{2,1,0:T(8,128)(2,1)S(1)}, bf16[1,1024,896]{2,1,0:T(8,128)(2,1)}, u32[]{:S(2)}) copy-start(bf16[1,1024,896]{2,1,0:T(8,128)(2,1)} %up_hbm.1) | copy-start | bytes 5505028
  3.7 1.5 %copy-start.2 = (bf16[1,896,1024]{2,1,0:T(8,128)(2,1)S(1)}, bf16[1,896,1024]{2,1,0:T(8,128)(2,1)}, u32[]{:S(2)}) copy-start(bf16[1,896,1024]{2,1,0:T(8,128)(2,1)} %down_hbm.1) | copy-start | bytes 5505028
  5.2 0.9 %copy-start.3 = (bf16[128,1024]{1,0:T(8,128)(2,1)S(1)}, bf16[128,1024]{1,0:T(8,128)(2,1)}, u32[]{:S(2)}) copy-start(bf16[128,1024]{1,0:T(8,128)(2,1)} %tok_ref.1) | copy-start | bytes 786436
  6.2 0.7 copy-start.4

commit v2 on v1

--- a/solution.py
+++ b/solution.py
@@ -9,7 +9,7 @@
 
 TOP_K = 2
 MESH = pl.DeviceIdType.MESH
-VMEM_ROOM = 48 << 20
+VMEM_ROOM = 60 << 20
 
 
 def norm_rows(tokens, norm_gain):
@@ -160,7 +160,7 @@
         return remote(tbuf.at[dz - 1], zrecv.at[n - dz - 1], rsz_s.at[dz], rsz_r.at[n - dz], along(dz))
 
     ag_y(0).start()
-    for k in range(1, n):
+    for k in reversed(range(1, n)):
         ag_z(k).start()
     for k in range(1, 4):
         share(k).start()

time: 84.1 us -> 76.4 us (0.908)
  the two profiles are of different devices: /device:TPU:0 before, /device:TPU:25 now
where the time goes in v2:
time: 76.4 us; the launch traced here: 76.2 us
  Pallas kernels  73.1 us (96%)
  local copies, waits for them, and re-layouts  2.28 us (3%)
    pallas_call x1, Pallas kernels, fused_body(): pl.pallas_call(functools.partial(kernel, n), out_shape=jax.ShapeDtypeStru...  73.1 us
    unnamed x1, local copies, waits for them, and re-layouts  1.67 us

profile of v2, /device:TPU:25, one launch (start us, length us, event | category | flops | bytes accessed | tf_op | source)
XLA Modules:
  0.0 76.2 jit_solution(6991520795850281403)
XLA Ops:
  0.0 0.7 select_reduce_fusion
  0.7 0.6 reshape.9.share_ref
  1.3 73.1 %shard_map.73 = bf16[128,1024]{1,0:T(8,128)(2,1)} custom-call(bf16[128,1024]{1,0:T(8,128)(2,1)} %tok_ref.1, f32[1,1024]{1,0:T(1,128)} %bitcast.1, f32[4,4,128]{2,1,0:T(4,128)} %reshape.9.share_ref, bf16[1,1024,896]{2,1,0:T(8,128)(2,1)} %gate_hbm.1, bf16[1,1024,896]{2,1,0:T(8,128)(2,1)} %up_hbm.1, bf16[1,896,1024]{2,1,0:T(8,128)(2,1)} %down_hbm.1), custom_call_target="tpu_custom_call" | custom-call | tf_op jit(solution)/shard_map/pallas_call | solution.py:271
  74.5 1.7 %copy.11 = bf16[128,1024]{1,0:T(8,128)(2,1)} copy(bf16[128,1024]{1,0:T(8,128)(2,1)} %shard_map.73) | data formatting | bytes 524288
